TPU v7x, 32 devices: a whole 2x2x4 slice. The times are simulated.
32 devices in a mesh: sp: 8 (over z, core), tp: 4 (over y, x).
Axes of the slice: x: 2, y: 2, z: 4, core: 2. Of those that a mesh axis runs over, the one named last changes fastest.
Arguments:
- queries: bfloat16 [2048, 2048], P('sp', 'tp'), may hold values from -8 to 8
- key_rows: bfloat16 [2048, 1024], P('sp', 'tp'), may hold values from -8 to 8
- values: bfloat16 [2048, 1024], P('sp', 'tp'), may hold values from -6 to 6
- sink_logits: float32 [32], P('tp'), may hold values from 2 to 6
- residual: bfloat16 [2048, 2048], P(('sp', 'tp')), may hold values from -6 to 6
- out_weight: bfloat16 [2048, 2048], P('tp'), may hold values from -0.125 to 0.125
- norm_gain: float32 [2048], replicated, may hold values from 0.1 to 1.9
- expert_ids: int32 [2048, 2], P('sp'), may hold values from 0 to 7, as said below
- route_weight: float32 [2048, 2], P('sp'), may hold values from 0.2 to 1
- gate_proj: bfloat16 [8, 2048, 4096], P('sp', None, 'tp'), may hold values from -0.125 to 0.125
- up_proj: bfloat16 [8, 2048, 4096], P('sp', None, 'tp'), may hold values from -0.125 to 0.125
- down_proj: bfloat16 [8, 4096, 2048], P('sp', 'tp'), may hold values from -0.09375 to 0.09375
Outputs:
- mixed_out: bfloat16 [2048, 2048], P(('sp', 'tp'))
Inputs may be any that keep to these rules, and one draw needn't show every extreme that they name: `expert_ids`: the two entries of a row are different experts of one group: experts g * 2 to g * 2 + 1 for a group g below 4. In each aligned block of 64 rows (the rows of one device) no expert is named more than 32 times, and one expert is named exactly 32 times in every block.
All inputs are finite; a program needn't handle non-finite values.
Results may differ from a plain program's by a relative error of at most 0.014.
Values may be sent and summed in bfloat16 or wider, within the bound.
A program may use at most 64 MiB of HBM per device.

v0:
```python
import jax
import jax.numpy as jnp
from jax import lax
from jax.sharding import PartitionSpec as P

HEAD = 64
WINDOW = 128


norm_epsilon = 1e-06


def from_behind(block, axis, distance):
    devices = range(lax.axis_size(axis))
    route = [(i - distance, i) for i in devices if i - distance in devices]
    return lax.ppermute(block, axis, route)


def rotary(values_in, positions, head_count):
    halfway = HEAD // 2
    frequency = 10000.0 ** (-jnp.arange(halfway, dtype=jnp.float32) * 2.0 / HEAD)
    angles = positions.astype(jnp.float32)[:, None] * frequency[None, :]
    cosine = jnp.cos(angles)[:, None, :]
    sine_part = jnp.sin(angles)[:, None, :]
    reshaped = values_in.astype(jnp.float32).reshape(values_in.shape[0], head_count, HEAD)
    front_part = reshaped[..., :halfway]
    back_part = reshaped[..., halfway:]
    turned = jnp.concatenate(
        [front_part * cosine - back_part * sine_part, back_part * cosine + front_part * sine_part],
        -1,
    )
    return turned.astype(jnp.bfloat16)


def attend(query_blocks, key_pairs, value_pairs, sink_grid, key_start):
    block_count = query_blocks.shape[0]
    window_len = query_blocks.shape[1]
    scores = jnp.einsum(
        "bqkgd,bskd->bkgqs", query_blocks, key_pairs, preferred_element_type=jnp.float32
    ) * HEAD ** (-0.5)
    row_idx = jnp.arange(window_len)[:, None]
    col_idx = jnp.arange(2 * window_len)[None, :]
    distance = row_idx - col_idx + window_len
    key_pos = key_start + jnp.arange(block_count)[:, None, None] * window_len + col_idx[None]
    allowed = (distance >= 0)[None] & (distance < window_len)[None] & (key_pos >= 0)
    scores = jnp.where(allowed[:, None, None], scores, -jnp.inf)
    sink_full = sink_grid[None, :, :, None]
    highest = jnp.maximum(jnp.max(scores, -1), sink_full)
    exp_scores = jnp.exp(scores - highest[..., None])
    denominator = jnp.sum(exp_scores, -1) + jnp.exp(sink_full - highest)
    weighted = jnp.einsum(
        "bkgqs,bskd->bkgqd",
        exp_scores.astype(jnp.bfloat16),
        value_pairs,
        preferred_element_type=jnp.float32,
    )
    normalized = weighted / denominator[..., None]
    return (
        jnp.transpose(normalized, (0, 3, 1, 2, 4))
        .astype(jnp.bfloat16)
        .reshape(block_count * window_len, -1)
    )


def slot_select(picks_in, expert_count, capacity):
    flattened = picks_in.reshape(-1)
    onehot = (flattened[:, None] == jnp.arange(expert_count, dtype=jnp.int32)[None, :]).astype(
        jnp.int32
    )
    rank_of = jnp.sum(jnp.cumsum(onehot, 0) * onehot, 1) - 1
    slot_of = flattened * capacity + rank_of
    chosen = jnp.arange(expert_count * capacity, dtype=jnp.int32)[:, None] == slot_of[None, :]
    return chosen.astype(jnp.bfloat16)


def expert_part(rows_in, gate_proj, up_proj, down_proj):
    in_shape = rows_in.shape
    flattened = rows_in.reshape(-1, in_shape[-1])
    gate_val = jnp.dot(flattened, gate_proj[0], preferred_element_type=jnp.float32)
    up_val = jnp.dot(flattened, up_proj[0], preferred_element_type=jnp.float32)
    hidden = (jax.nn.silu(gate_val) * up_val).astype(jnp.bfloat16)
    return (
        jnp.dot(hidden, down_proj[0], preferred_element_type=jnp.float32)
        .astype(jnp.bfloat16)
        .reshape(in_shape)
    )


def per_device(
    queries,
    key_rows,
    values,
    sink_logits,
    residual,
    out_weight,
    norm_gain,
    expert_ids,
    route_weight,
    gate_proj,
    up_proj,
    down_proj,
):
    local_len = queries.shape[0]
    q_heads = sink_logits.shape[0]
    kv_heads = key_rows.shape[1] // HEAD
    group_size = q_heads // kv_heads
    window_len = WINDOW
    seq_start = lax.axis_index("sp") * local_len
    rim_pair = jnp.stack([key_rows[local_len - window_len :], values[local_len - window_len :]])
    rim_pair = from_behind(rim_pair, "sp", 1)
    key_ext = jnp.concatenate([rim_pair[0], key_rows], 0)
    val_ext = jnp.concatenate([rim_pair[1], values], 0)
    positions = seq_start + jnp.arange(local_len, dtype=jnp.int32)
    ext_positions = seq_start - window_len + jnp.arange(local_len + window_len, dtype=jnp.int32)
    rot_query = rotary(queries, positions, q_heads)
    rot_key = rotary(key_ext, ext_positions, kv_heads)
    block_count = local_len // window_len
    query_blocks = rot_query.reshape(block_count, window_len, kv_heads, group_size, HEAD)
    key_blocks = rot_key.reshape(block_count + 1, window_len, kv_heads, HEAD)
    value_blocks = val_ext.reshape(block_count + 1, window_len, kv_heads, HEAD)
    key_pairs = jnp.concatenate([key_blocks[:-1], key_blocks[1:]], 1)
    value_pairs = jnp.concatenate([value_blocks[:-1], value_blocks[1:]], 1)
    sink_grid = sink_logits.reshape(kv_heads, group_size)
    attended = attend(query_blocks, key_pairs, value_pairs, sink_grid, seq_start - window_len)
    tok_rows = residual.shape[0]
    tp_count = lax.axis_size("tp")
    tp_index = lax.axis_index("tp")
    projected = lax.psum_scatter(
        jnp.dot(attended, out_weight, preferred_element_type=jnp.float32).astype(jnp.bfloat16),
        "tp",
        scatter_dimension=0,
        tiled=True,
    ).astype(jnp.float32)
    middle = (residual.astype(jnp.float32) + projected).astype(jnp.bfloat16)
    middle_f = middle.astype(jnp.float32)
    normed = (
        middle_f
        * lax.rsqrt(jnp.mean(middle_f * middle_f, -1, keepdims=True) + norm_epsilon)
        * norm_gain
    ).astype(jnp.bfloat16)
    expert_count = lax.axis_size("sp")
    capacity = 2 * max(1, 2 * tok_rows // expert_count)
    model_width = normed.shape[1]
    own_ids = lax.dynamic_slice_in_dim(expert_ids, tp_index * tok_rows, tok_rows, 0)
    own_weights = lax.dynamic_slice_in_dim(route_weight, tp_index * tok_rows, tok_rows, 0)
    select = slot_select(own_ids, expert_count, capacity)
    token_select = jnp.sum(select.reshape(expert_count * capacity, tok_rows, 2), -1)
    outbound = jnp.dot(token_select, normed, preferred_element_type=jnp.float32).astype(
        jnp.bfloat16
    )
    outbound = outbound.reshape(expert_count, capacity, model_width)
    arrived = lax.all_to_all(outbound, "sp", split_axis=0, concat_axis=0, tiled=True)
    partial_out = expert_part(
        lax.all_gather(arrived, "tp", axis=0, tiled=True), gate_proj, up_proj, down_proj
    )
    partial_out = partial_out.reshape(tp_count, expert_count * capacity, model_width)
    width_parts = lax.all_to_all(partial_out, "tp", split_axis=0, concat_axis=0, tiled=True)
    summed = jnp.sum(width_parts.astype(jnp.float32), 0).reshape(
        expert_count, capacity, model_width
    )
    returned = (
        lax.all_to_all(summed.astype(jnp.bfloat16), "sp", split_axis=0, concat_axis=0, tiled=True)
        .astype(summed.dtype)
        .reshape(expert_count * capacity, model_width)
    )
    picked = jnp.dot(
        select.astype(jnp.float32).T,
        returned,
        precision=lax.Precision.HIGHEST,
        preferred_element_type=jnp.float32,
    )
    routed = jnp.sum(picked.reshape(tok_rows, 2, model_width) * own_weights[..., None], 1)
    return (middle_f + routed).astype(jnp.bfloat16)


def solution(mesh):
    return jax.shard_map(
        per_device,
        mesh=mesh,
        in_specs=(
            P("sp", "tp"),
            P("sp", "tp"),
            P("sp", "tp"),
            P("tp"),
            P(("sp", "tp"), None),
            P("tp", None),
            P(),
            P("sp", None),
            P("sp", None),
            P("sp", None, "tp"),
            P("sp", None, "tp"),
            P("sp", "tp", None),
        ),
        out_specs=P(("sp", "tp"), None),
        check_vma=False,
    )
```

profile of v0, /device:TPU:0, one launch (start us, length us, event | category | flops | bytes accessed | tf_op | source)
XLA Modules:
  0.0 250.8 jit_solution(17976046519329344220)
XLA Ops:
  6.5 1.2 copy.49
  7.7 0.8 slice.47
  8.7 2.4 collective-permute-start
  11.2 1.1 reshape.279
  12.3 0.3 multiply_cosine_fusion
  12.6 0.2 multiply_cosine_fusion.1
  12.8 1.1 copy.54
  14.3 0.2 copy.61
  14.8 0.5 fusion.46
  15.5 1.3 copy-done.2
  16.7 0.3 fusion.11
  17.3 0.2 reshape.278
  17.4 0.2 copy.60
  17.6 2.1 fusion.15
  19.7 0.3 copy.63
  20.0 1.7 convolution_convert_fusion
  22.2 0.2 reduce_window_sum.11
  22.4 0.2 select_reduce_fusion
  22.9 30.0 %reduce-scatter.2.cloned.1.call-done = bf16[64,2048]{1,0:T(8,128)(2,1)} async-done(((bf16[256,2048]{1,0:T(8,128)(2,1)}), bf16[64,2048]{1,0:T(8,128)(2,1)}) %reduce-scatter.2.cloned.1.call-update) | async-done | bytes 262160 | tf_op jit(solution)/shard_map/reduce_scatter | solution.py:128
  52.9 1.1 fusion.18
  54.1 1.4 convolution_convert_fusion.1
  55.5 31.1 %all_to_all.15 = bf16[8,32,2048]{2,1,0:T(8,128)(2,1)} all-to-all(bf16[8,32,2048]{2,1,0:T(8,128)(2,1)S(1)} %bitcast.78), channel_id=1, replica_groups=mesh['sp'=8,'tp'=4] {'sp'}, dimensions={0} | all-to-all | bytes 2097152 | tf_op jit(solution)/shard_map/all_to_all | solution.py:152
  86.6 50.7 %all-gather.2.cloned.1.call-done = bf16[32,32,2048]{2,1,0:T(8,128)(2,1)} async-done(((bf16[8,32,2048]{2,1,0:T(8,128)(2,1)}), bf16[32,32,2048]{2,1,0:T(8,128)(2,1)}) %all-gather.2.cloned.1.call-update) | async-done | bytes 4194320 | tf_op jit(solution)/shard_map/all_gather | solution.py:154
  137.3 7.7 %fusion.2 = f32[1024,1024]{1,0:T(8,128)S(1)} fusion(bf16[1024,2048]{1,0:T(8,128)(2,1)} %bitcast.85, bf16[1,2048,1024]{2,1,0:T(8,128)(2,1)} %param.22), kind=kOutput, calls=%fused_computation.2 | convolution fusion | flops 4294967296 | bytes 12582912 | tf_op jit(solution)/shard_map/dot_general | solution.py:80
  145.0 5.4 %multiply_convert_fusion = bf16[1024,1024]{1,0:T(8,128)(2,1)S(1)} fusion(f32[1024,1024]{1,0:T(8,128)S(1)} %fusion.2, bf16[1024,2048]{1,0:T(8,128)(2,1)S(1)} %bitcast.86, bf16[1,2048,1024]{2,1,0:T(8,128)(2,1)S(1)} %copy-done.8), kind=kOutput, calls=%fused_computation.6 | convolution fusion | flops 4301258752 | bytes 14680064 | tf_op jit(solution)/shard_map/dot_general | solution.py:79
  150.4 4.7 %fusion.6 = bf16[1024,2048]{1,0:T(8,128)(2,1)S(1)} fusion(bf16[1024,1024]{1,0:T(8,128)(2,1)S(1)} %multiply_convert_fusion, bf16[1,1024,2048]{2,1,0:T(8,128)(2,1)S(1)} %copy-done.9), kind=kOutput, calls=%fused_computation.7 | convolution fusion | flops 4297064448 | bytes 10485760 | tf_op jit(solution)/shard_map/dot_general | solution.py:83
  155.1 51.4 %all_to_all.16 = bf16[4,256,2048]{2,1,0:T(8,128)(2,1)} all-to-all(bf16[4,256,2048]{2,1,0:T(8,128)(2,1)S(1)} %bitcast.76), channel_id=1, replica_groups=mesh['sp'=8,'tp'=4] {'tp'}, dimensions={0} | all-to-all | bytes 8388608 | tf_op jit(solution)/shard_map/all_to_all | solution.py:157
  206.5 4.3 %reduce_sum.64 = bf16[256,2048]{1,0:T(8,128)(2,1)} reduce(bf16[4,256,2048]{2,1,0:T(8,128)(2,1)} %all_to_all.16, bf16[]{:T(256)} %constant.52.clone.1), dimensions={0}, to_apply=%region_7.8 | reduce | flops 1572864 | bytes 5242882 | tf_op jit(solution)/shard_map/reduce_sum | solution.py:158
  210.7 4.6 %all-to-all-start.2 = ((bf16[8,32,2048]{2,1,0:T(8,128)(2,1)}), bf16[8,32,2048]{2,1,0:T(8,128)(2,1)S(1)}, u32[]{:S(2)}, u32[]{:S(2)}) async-start(bf16[8,32,2048]{2,1,0:T(8,128)(2,1)} %bitcast.79), calls=%async_computation.3 | async-start | bytes 2097152 | tf_op jit(solution)/shard_map/all_to_all | solution.py:162
  215.6 26.3 %all-to-all-done.2 = bf16[8,32,2048]{2,1,0:T(8,128)(2,1)S(1)} async-done(((bf16[8,32,2048]{2,1,0:T(8,128)(2,1)}), bf16[8,32,2048]{2,1,0:T(8,128)(2,1)S(1)}, u32[]{:S(2)}, u32[]{:S(2)}) %all-to-all-start.2) | async-done | bytes 1048608 | tf_op jit(solution)/shard_map/all_to_all | solution.py:162
  241.9 0.3 fusion.13
  242.2 1.7 fusion.21
  (65 shorter events, 2.2 us)
Async XLA Ops:
  6.5 13.5 %copy-start = (bf16[512,2048]{1,0:T(8,128)(2,1)S(1)}, bf16[512,2048]{1,0:T(8,128)(2,1)}, u32[]{:S(2)}) copy-start(bf16[512,2048]{1,0:T(8,128)(2,1)} %param.17) | copy-start | bytes 6291460
  6.5 7.7 %copy-start.5 = (f32[8]{0:T(128)S(1)}, f32[8]{0:T(128)}, u32[]{:S(2)}) copy-start(f32[8]{0:T(128)} %param.15) | copy-start | bytes 100
  6.5 46.4 %reduce-scatter.2.cloned.1.call-start = ((), (), s32[]{:S(2)}) async-start(), calls=%async_computation.4 | async-start | bytes 1310720 | tf_op jit(solution)/shard_map/reduce_scatter | solution.py:128
  8.7 5.9 %collective-permute-start = (bf16[2,128,256]{1,2,0:T(8,128)(2,1)S(1)}, bf16[2,128,256]{1,2,0:T(8,128)(2,1)S(1)}, u32[]{:S(2)}, u32[]{:S(2)}) collective-permute-start(bf16[2,128,256]{1,2,0:T(8,128)(2,1)S(1)} %pad_maximum_fusion.2), channel_id=1, source_target_pairs={{0,4},{4,8},{8,12},{12,16},{16,20},{20,24},{24,28},{1,5},{5,9},{9,... | collective-permute-start | bytes 393224 | tf_op jit(solution)/shard_map/ppermute | solution.py:16
  14.1 3.1 %copy-start.3 = (bf16[256,256]{1,0:T(8,128)(2,1)S(1)}, bf16[256,256]{1,0:T(8,128)(2,1)}, u32[]{:S(2)}) copy-start(bf16[256,256]{1,0:T(8,128)(2,1)} %param.14) | copy-start | bytes 393220
  15.4 1.3 copy-start.2
  17.6 4.2 %copy-start.6 = (s32[256,2]{0,1:T(2,128)S(1)}, s32[256,2]{0,1:T(2,128)}, u32[]{:S(2)}) copy-start(s32[256,2]{0,1:T(2,128)} %param.19) | copy-start | bytes 6148
  17.6 35.3 %copy-start.1 = (bf16[64,2048]{1,0:T(8,128)(2,1)S(1)}, bf16[64,2048]{1,0:T(8,128)(2,1)}, u32[]{:S(2)}) copy-start(bf16[64,2048]{1,0:T(8,128)(2,1)} %param.16) | copy-start | bytes 786436
  17.6 36.5 %copy-start.4 = (f32[2048]{0:T(1024)S(1)}, f32[2048]{0:T(1024)}, u32[]{:S(2)}) copy-start(f32[2048]{0:T(1024)} %param.18) | copy-start | bytes 24580
  21.7 115.6 %all-gather.2.cloned.1.call-start = ((), (), s32[]{:S(2)}) async-start(), calls=%async_computation.5 | async-start | bytes 5242880 | tf_op jit(solution)/shard_map/all_gather | solution.py:154
  137.3 7.7 %copy-start.8 = (bf16[1,2048,1024]{2,1,0:T(8,128)(2,1)S(1)}, bf16[1,2048,1024]{2,1,0:T(8,128)(2,1)}, u32[]{:S(2)}) copy-start(bf16[1,2048,1024]{2,1,0:T(8,128)(2,1)} %param.21) | copy-start | bytes 12582916
  137.3 7.7 %copy-start.10 = (bf16[32,32,2048]{2,1,0:T(8,128)(2,1)S(1)}, bf16[32,32,2048]{2,1,0:T(8,128)(2,1)}, u32[]{:S(2)}) copy-start(bf16[32,32,2048]{2,1,0:T(8,128)(2,1)} %all-gather.2.cloned.1.call-done) | copy-start | bytes 12582916
  145.0 5.4 %copy-start.9 = (bf16[1,1024,2048]{2,1,0:T(8,128)(2,1)S(1)}, bf16[1,1024,2048]{2,1,0:T(8,128)(2,1)}, u32[]{:S(2)}) copy-start(bf16[1,1024,2048]{2,1,0:T(8,128)(2,1)} %param.23) | copy-start | bytes 12582916
  206.5 9.0 %copy-start.7 = (f32[256,2]{0,1:T(2,128)S(1)}, f32[256,2]{0,1:T(2,128)}, u32[]{:S(2)}) copy-start(f32[256,2]{0,1:T(2,128)} %param.20) | copy-start | bytes 6148
  210.7 31.2 %all-to-all-start.2 = ((bf16[8,32,2048]{2,1,0:T(8,128)(2,1)}), bf16[8,32,2048]{2,1,0:T(8,128)(2,1)S(1)}, u32[]{:S(2)}, u32[]{:S(2)}) async-start(bf16[8,32,2048]{2,1,0:T(8,128)(2,1)} %bitcast.79), calls=%async_computation.3 | async-start | bytes 2097152 | tf_op jit(solution)/shard_map/all_to_all | solution.py:162
Sparse Core Ops, SparseCore 0:
  21.9 31.0 reduce-scatter.1
  86.7 50.5 all-gather.1
where the time goes:
time: 251 us
  waiting for transfers between devices  107 us (43%)
  blocking collectives  82.4 us (33%)
  matrix products  23.8 us (9%)
  between operations  13.9 us (6%)
  other arithmetic  9.23 us (4%)
  local copies, waits for them, and re-layouts  7.35 us (3%)
  starting transfers between devices  7.04 us (3%)
    all_to_all x1, blocking collectives, per_device(): lax.all_to_all(partial_out, 'tp', split_axis=0, concat_axis=0, tiled=True)  51.4 us
    all_gather x1, waiting for transfers between devices, per_device(): lax.all_gather(arrived, 'tp', axis=0, tiled=True)  50.7 us
    all_to_all x1, blocking collectives, per_device(): lax.all_to_all(outbound, 'sp', split_axis=0, concat_axis=0, tiled=True)  31.1 us
    reduce_scatter x1, waiting for transfers between devices, per_device(): lax.psum_scatter(jnp.dot(attended, out_weight, preferred_element_type=jnp...  30 us
    all_to_all x1, waiting for transfers between devices, per_device(): lax.all_to_all(summed.astype(jnp.bfloat16), 'sp', split_axis=0, concat_ax...  26.3 us
    dot_general x1, matrix products, expert_part(): up_val = jnp.dot(flattened, up_proj[0], preferred_element_type=jnp.float32)  7.65 us
    dot_general x1, matrix products, expert_part(): jnp.dot(flattened, gate_proj[0], preferred_element_type=jnp.float32)  5.35 us
  transfers between devices with their start and end apart: 4, of which 3 were waited for; matrix products, arithmetic and copies ran while one was open for 2% of the time, Pallas kernels for 0%

commit v1 on v0

--- a/solution.py
+++ b/solution.py
@@ -1,6 +1,8 @@
 import jax
 import jax.numpy as jnp
 from jax import lax
+from jax.experimental import pallas as pl
+from jax.experimental.pallas import tpu as pltpu
 from jax.sharding import PartitionSpec as P
 
 HEAD = 64
@@ -83,6 +85,284 @@
         jnp.dot(hidden, down_proj[0], preferred_element_type=jnp.float32)
         .astype(jnp.bfloat16)
         .reshape(in_shape)
+    )
+
+
+GROUPS = 4
+TILE = 256
+MESH = pl.DeviceIdType.MESH
+
+
+def group_kernel(
+    proj, resid, gain, extra, sel, sel_back, wg_hbm, wu_hbm, wd_hbm, out,
+    wg, wu, wd, w_sem,
+    rs_in, rs_s, rs_r,
+    mid, normed, outb, rows,
+    di_s, di_r, ag_s, ag_r, pt_s, pt_r,
+    hid, outp, pr, pr_s, pr_r,
+    comb, rs2, r2_s, r2_r,
+    ret, back, bk_s, bk_r,
+):
+    sp = lax.axis_index("sp")
+    t = lax.axis_index("tp")
+    core = lax.rem(sp, 2)
+    z = sp // 2
+    tp_n, row_n, width = proj.shape
+    ext_width = normed.shape[1]
+    cap = outb.shape[1]
+    half = GROUPS * cap
+    flip1 = t + 1 - 2 * lax.rem(t, 2)
+    flip2 = lax.rem(t + 2, 4)
+    flip3 = lax.rem(flip1 + 2, 4)
+    peer = [t, flip1, flip2, flip3]
+    partner = sp + 1 - 2 * core
+    zoff = lambda k: lax.rem(z + k + GROUPS, GROUPS)
+
+    loads = [
+        pltpu.make_async_copy(a, b, w_sem.at[i])
+        for i, (a, b) in enumerate(((wg_hbm, wg), (wu_hbm, wu), (wd_hbm, wd)))
+    ]
+    for c in loads:
+        c.start()
+
+    barrier = pltpu.get_barrier_semaphore()
+    friends = [(sp, peer[d]) for d in (1, 2, 3)]
+    friends += [(zoff(k) * 2 + core, t) for k in (1, 2, 3)] + [(partner, t)]
+    for dev in friends:
+        pl.semaphore_signal(barrier, inc=1, device_id=dev, device_id_type=MESH)
+    pl.semaphore_wait(barrier, len(friends))
+
+    sent = []
+
+    def send(src, dst, ss, rs, dev):
+        c = pltpu.make_async_remote_copy(
+            src_ref=src, dst_ref=dst, send_sem=ss, recv_sem=rs, device_id=dev, device_id_type=MESH
+        )
+        c.start()
+        sent.append(c)
+        return c
+
+    firsts = [
+        send(proj.at[peer[d]], rs_in.at[d - 1], rs_s.at[d - 1], rs_r.at[d - 1], (sp, peer[d]))
+        for d in (3, 1, 2)
+    ]
+    for c in firsts:
+        c.wait_recv()
+    total = resid[...].astype(jnp.float32) + (
+        proj[t].astype(jnp.float32)
+        + rs_in[0].astype(jnp.float32)
+        + rs_in[1].astype(jnp.float32)
+        + rs_in[2].astype(jnp.float32)
+    )
+    middle = total.astype(jnp.bfloat16)
+    mid[...] = middle
+    mf = middle.astype(jnp.float32)
+    scale = lax.rsqrt(jnp.mean(mf * mf, -1, keepdims=True) + norm_epsilon)
+    normed[:, :width] = (mf * scale * gain[...]).astype(jnp.bfloat16)
+    normed[:, width:] = extra[...]
+
+    def block(tt, cc, zz):
+        return rows.at[tt, pl.ds(pl.multiple_of((cc * GROUPS + zz) * cap, cap), cap)]
+
+    def pack(g):
+        s = sel[pl.ds(pl.multiple_of(g * cap, cap), cap), :]
+        return jnp.dot(s, normed[...], preferred_element_type=jnp.float32).astype(jnp.bfloat16)
+
+    disp = [None] * GROUPS
+    for k in (2, 1, 3):
+        g = zoff(k)
+        outb[k] = pack(g)
+        disp[k] = send(
+            outb.at[k], block(t, core, z), di_s.at[k - 1], di_r.at[k - 1], (2 * g + core, t)
+        )
+    block(t, core, z)[...] = pack(z)
+
+    ag = {}
+    pt = {}
+
+    def push(d, k, tt, to):
+        ref = block(tt, core, zoff(-k))
+        ag[(d, k)] = send(ref, ref, ag_s.at[d - 1, k], ag_r.at[d - 1, k], (sp, peer[to]))
+
+    def across(d, k):
+        ref = block(peer[d], core, zoff(-k))
+        pt[(d, k)] = send(ref, ref, pt_s.at[d, k], pt_r.at[d, k], (partner, t))
+
+    order = (0, 1, 3, 2)
+
+    def relay(i):
+        k = order[i]
+        ag[(1, k)].wait_recv()
+        if i < 2:
+            push(3, k, peer[1], 2)
+        across(1, k)
+        ag[(2, k)].wait_recv()
+        if i >= 2:
+            push(3, k, peer[2], 1)
+        across(2, k)
+
+    for i, k in enumerate(order):
+        if k:
+            disp[k].wait_recv()
+        push(1, k, t, 1)
+        push(2, k, t, 2)
+        across(0, k)
+        if i:
+            relay(i - 1)
+
+    for c in loads:
+        c.wait()
+
+    def experts(d):
+        for k in order:
+            pt[(d, k)].wait_recv()
+        tt = peer[d]
+
+        @pl.loop(0, wg.shape[1] // TILE)
+        def _(n):
+            cols = pl.ds(pl.multiple_of(n * TILE, TILE), TILE)
+            x = rows[tt, :, :width]
+            g = jnp.dot(x, wg[:, cols], preferred_element_type=jnp.float32)
+            u = jnp.dot(x, wu[:, cols], preferred_element_type=jnp.float32)
+            hid[:, cols] = (g / (1.0 + jnp.exp(-g)) * u).astype(jnp.bfloat16)
+
+        ext = rows[tt, :, width:].astype(jnp.float32)
+        lane = lax.broadcasted_iota(jnp.int32, ext.shape, 1)
+        mine = (lane == core) | (lane == core + 2)
+        weight = jnp.sum(jnp.where(mine, ext, 0.0), -1, keepdims=True)
+
+        @pl.loop(0, width // TILE)
+        def _(n):
+            cols = pl.ds(pl.multiple_of(n * TILE, TILE), TILE)
+            y = jnp.dot(hid[...], wd[:, cols], preferred_element_type=jnp.float32)
+            outp[d, :, cols] = (y * weight).astype(jnp.bfloat16)
+
+        src = outp.at[d, pl.ds(pl.multiple_of((1 - core) * half, half), half)]
+        return send(src, pr.at[d], pr_s.at[d], pr_r.at[d], (partner, t))
+
+    def own(d, zz):
+        off = pl.multiple_of((core * GROUPS + zz) * cap, cap)
+        here = pl.ds(pl.multiple_of(zz * cap, cap), cap)
+        return outp[d, pl.ds(off, cap), :].astype(jnp.float32) + pr[d, here, :].astype(jnp.float32)
+
+    back_order = (2, 1, 3, 0)
+    r2 = {}
+
+    def combine(d, swap):
+        swap.wait_recv()
+        for k in back_order:
+            zz = zoff(-k)
+            comb[d - 1, k] = own(d, zz).astype(jnp.bfloat16)
+            r2[(d, k)] = send(
+                comb.at[d - 1, k], rs2.at[d - 1, k],
+                r2_s.at[d - 1, k], r2_r.at[d - 1, k], (sp, peer[d]),
+            )
+
+    swap0 = experts(0)
+    relay(3)
+    swap1 = experts(1)
+    swap0.wait_recv()
+    for k in order:
+        ag[(3, k)].wait_recv()
+        across(3, k)
+    combine(1, swap1)
+    swap2 = experts(2)
+    combine(2, swap2)
+    swap3 = experts(3)
+    combine(3, swap3)
+
+    bk = []
+    for k in back_order:
+        zz = zoff(-k)
+        acc = own(0, zz)
+        for d in (1, 2, 3):
+            r2[(d, k)].wait_recv()
+            acc = acc + rs2[d - 1, k].astype(jnp.float32)
+        if k:
+            ret[k] = acc.astype(jnp.bfloat16)
+            bk.append(
+                send(ret.at[k], back.at[z], bk_s.at[k - 1], bk_r.at[k - 1], (2 * zz + core, t))
+            )
+        else:
+            back[z] = acc.astype(jnp.bfloat16)
+    for c in bk:
+        c.wait_recv()
+    routed = jnp.dot(
+        sel_back[...], back[...].reshape(half, width), preferred_element_type=jnp.float32
+    )
+    out[...] = (mid[...].astype(jnp.float32) + routed).astype(jnp.bfloat16)
+    for c in sent:
+        c.wait_send()
+
+
+def group_experts(projected, residual, norm_gain, own_ids, own_weights, gate, up, down):
+    row_n, width = residual.shape
+    tp_n = lax.axis_size("tp")
+    expert_n = lax.axis_size("sp")
+    cap = 2 * max(1, 2 * row_n // expert_n)
+    group = own_ids[:, 0] // 2
+    onehot = (group[:, None] == jnp.arange(GROUPS, dtype=jnp.int32)[None, :]).astype(jnp.int32)
+    rank_of = jnp.sum(jnp.cumsum(onehot, 0) * onehot, 1) - 1
+    slot = group * cap + rank_of
+    hit = jnp.arange(GROUPS * cap, dtype=jnp.int32)[:, None] == slot[None, :]
+    sel = hit.astype(jnp.bfloat16)
+    odd = lax.rem(own_ids, 2)
+    pair = jnp.stack(
+        [jnp.sum(jnp.where(odd == p, own_weights, 0.0), 1) for p in (0, 1)], 1
+    )
+    high = pair.astype(jnp.bfloat16)
+    low = (pair - high.astype(jnp.float32)).astype(jnp.bfloat16)
+    extra = jnp.pad(jnp.concatenate([high, low], 1), ((0, 0), (0, 124)))
+    ext_width = width + 128
+    ff = gate.shape[-1]
+    half = GROUPS * cap
+    bf = jnp.bfloat16
+    dma = pltpu.SemaphoreType.DMA
+    vmem = pl.BlockSpec(memory_space=pltpu.VMEM)
+    hbm = pl.BlockSpec(memory_space=pl.ANY)
+    return pl.pallas_call(
+        group_kernel,
+        out_shape=jax.ShapeDtypeStruct((row_n, width), bf),
+        in_specs=[vmem] * 6 + [hbm] * 3,
+        out_specs=vmem,
+        scratch_shapes=[
+            pltpu.VMEM((width, ff), bf),
+            pltpu.VMEM((width, ff), bf),
+            pltpu.VMEM((ff, width), bf),
+            dma((3,)),
+            pltpu.VMEM((3, row_n, width), bf),
+            dma((3,)),
+            dma((3,)),
+            pltpu.VMEM((row_n, width), bf),
+            pltpu.VMEM((row_n, ext_width), bf),
+            pltpu.VMEM((GROUPS, cap, ext_width), bf),
+            pltpu.VMEM((tp_n, 2 * half, ext_width), bf),
+            dma((3,)),
+            dma((3,)),
+            dma((3, GROUPS)),
+            dma((3, GROUPS)),
+            dma((4, GROUPS)),
+            dma((4, GROUPS)),
+            pltpu.VMEM((2 * half, ff), bf),
+            pltpu.VMEM((4, 2 * half, width), bf),
+            pltpu.VMEM((4, half, width), bf),
+            dma((4,)),
+            dma((4,)),
+            pltpu.VMEM((3, GROUPS, cap, width), bf),
+            pltpu.VMEM((3, GROUPS, cap, width), bf),
+            dma((3, GROUPS)),
+            dma((3, GROUPS)),
+            pltpu.VMEM((GROUPS, cap, width), bf),
+            pltpu.VMEM((GROUPS, cap, width), bf),
+            dma((3,)),
+            dma((3,)),
+        ],
+        compiler_params=pltpu.CompilerParams(
+            collective_id=0, has_side_effects=True, vmem_limit_bytes=56 * 2**20
+        ),
+    )(
+        projected.reshape(tp_n, row_n, width), residual, norm_gain[None], extra, sel,
+        sel.T, gate[0], up[0], down[0],
     )
 
 
@@ -125,6 +405,19 @@
     tok_rows = residual.shape[0]
     tp_count = lax.axis_size("tp")
     tp_index = lax.axis_index("tp")
+    if tp_count == 4 and lax.axis_size("sp") == 2 * GROUPS:
+        return group_experts(
+            jnp.dot(attended, out_weight, preferred_element_type=jnp.float32).astype(
+                jnp.bfloat16
+            ),
+            residual,
+            norm_gain,
+            lax.dynamic_slice_in_dim(expert_ids, tp_index * tok_rows, tok_rows, 0),
+            lax.dynamic_slice_in_dim(route_weight, tp_index * tok_rows, tok_rows, 0),
+            gate_proj,
+            up_proj,
+            down_proj,
+        )
     projected = lax.psum_scatter(
         jnp.dot(attended, out_weight, preferred_element_type=jnp.float32).astype(jnp.bfloat16),
         "tp",

time: 251 us -> 113 us (0.45)
  waiting for transfers between devices: 107 us -> 0.01 us
  Pallas kernels: 0 us -> 90.2 us
  blocking collectives: 82.4 us -> 0 us
  matrix products: 23.8 us -> 4.3 us
  between operations: 13.9 us -> 0.31 us
  other arithmetic: 9.23 us -> 3.97 us
  starting transfers between devices: 7.04 us -> 2.4 us
    pallas_call x0 -> x1, Pallas kernels: none -> 90.2 us  [group_experts(): pl.pallas_call(group_kernel, out_shape=jax.ShapeDtypeStruct((row_n, width...]
    all_to_all x2 -> x0, blocking collectives: 82.4 us -> none  [the longest x1 51.4 us: per_device(): lax.all_to_all(partial_out, 'tp', split_axis=0, concat_axis=0, tiled=True)]
    all_gather x1 -> x0, waiting for transfers between devices: 50.7 us -> none  [per_device(): lax.all_gather(arrived, 'tp', axis=0, tiled=True)]
    reduce_scatter x1 -> x0, waiting for transfers between devices: 30 us -> none  [per_device(): lax.psum_scatter(jnp.dot(attended, out_weight, preferred_element_type=jnp...]
    all_to_all x1 -> x0, waiting for transfers between devices: 26.3 us -> none  [per_device(): lax.all_to_all(summed.astype(jnp.bfloat16), 'sp', split_axis=0, concat_ax...]
    dot_general x5 -> x0, matrix products: 19.5 us -> none  [the longest x1 7.65 us: expert_part(): up_val = jnp.dot(flattened, up_proj[0], preferred_element_type=jnp.float32)]
    reduce_sum x4 -> x2, other arithmetic: 5.66 us -> 0.97 us  [the longest x1 0.79 us: group_experts(): jnp.sum(jnp.where(odd == p, own_weights, 0.0), 1)]
    all_to_all x1 -> x0, starting transfers between devices: 4.6 us -> none  [per_device(): lax.all_to_all(summed.astype(jnp.bfloat16), 'sp', split_axis=0, concat_ax...]
  transfers between devices with their start and end apart: 4 -> 1, of which waited for: 3 -> 0; matrix products, arithmetic and copies ran while one was open for 2% -> 7% of each run, Pallas kernels for 0% -> 0%
where the time goes in v1:
time: 113 us; the launch traced here: 111 us
  Pallas kernels  90.2 us (80%)
  local copies, waits for them, and re-layouts  9.82 us (9%)
  matrix products  4.3 us (4%)
  other arithmetic  3.97 us (4%)
  starting transfers between devices  2.4 us (2%)
    pallas_call x1, Pallas kernels, group_experts(): pl.pallas_call(group_kernel, out_shape=jax.ShapeDtypeStruct((row_n, width...  90.2 us
    unnamed x12, local copies, waits for them, and re-layouts  5.3 us
    ppermute x1, starting transfers between devices, from_behind(): return lax.ppermute(block, axis, route)  2.4 us
  transfers between devices with their start and end apart: 1, of which 0 were waited for; matrix products, arithmetic and copies ran while one was open for 7% of the time, Pallas kernels for 0%

profile of v1, /device:TPU:0, one launch (start us, length us, event | category | flops | bytes accessed | tf_op | source)
XLA Modules:
  0.0 111.0 jit_solution(3813450774269699924)
XLA Ops:
  0.0 1.1 %copy.33 = bf16[256,256]{0,1:T(8,128)(2,1)S(1)} copy(bf16[256,256]{1,0:T(8,128)(2,1)} %param.13) | data formatting | bytes 262144 | tf_op args[1]
  1.2 0.8 slice.50
  2.0 0.1 copy.56
  2.2 2.4 %collective-permute-start = (bf16[2,128,256]{1,2,0:T(8,128)(2,1)S(1)}, bf16[2,128,256]{1,2,0:T(8,128)(2,1)S(1)}, u32[]{:S(2)}, u32[]{:S(2)}) collective-permute-start(bf16[2,128,256]{1,2,0:T(8,128)(2,1)S(1)} %pad_maximum_fusion.2), channel_id=1, source_target_pairs={{0,4},{4,8},{8,12},{12,16},{16,20},{20,24},{24,28},{1,5},{5,9},{9,... | collective-permute-start | bytes 393224 | tf_op jit(solution)/shard_map/ppermute | solution.py:18
  4.7 1.1 reshape.239
  5.8 0.8 fusion.24
  6.6 0.8 constant_dynamic-slice_fusion
  7.4 0.3 multiply_cosine_fusion
  7.6 0.2 multiply_cosine_fusion.1
  7.8 1.1 copy.38
  9.0 0.1 subtract_convert_fusion
  9.3 0.1 max.19
  9.3 0.2 copy.45
  9.5 0.1 copy.48
  9.7 0.1 reduce_window_sum.11
  9.8 0.2 select_reduce_fusion
  10.0 0.6 fusion.21.sel
  10.6 0.1 broadcast_and_fusion
  10.8 0.6 pad.4.extra
  11.4 0.7 fusion.23.sel_back
  12.3 0.5 fusion.31
  12.9 1.3 %copy-done.1 = f32[2,4,2,128,256]{3,4,2,1,0:T(8,128)} copy-done((f32[2,4,2,128,256]{3,4,2,1,0:T(8,128)}, f32[2,4,2,128,256]{3,4,2,1,0:T(8,128)S(1)}, u32[]{:S(2)}) %copy-start.1) | copy-done | bytes 2097176
  14.2 0.3 fusion
  14.5 0.1 add_bitcast_fusion
  14.6 0.1 copy.41
  14.7 0.2 reshape.238
  14.9 0.2 copy.44
  15.1 2.1 %fusion.3 = bf16[2,128,4,2,64]{1,4,3,2,0:T(8,128)(2,1)S(1)} fusion(f32[2,4,2,128,256]{3,4,2,1,0:T(8,128)} %copy-done.1, f32[2,4,2,128]{3,2,1,0:T(2,128)S(1)} %broadcast_maximum_fusion, bf16[2,128,4,64]{1,3,2,0:T(8,128)(2,1)S(1)} %copy.45, bf16[2,128,4,64]{1,3,2,0:T(8,128)(2,1)S(1)} %copy.44, f32[2,128,4,2]{1,3,2,0:T(2,128)S(1)} %add_bitcast_fusion), kind=kOutput, calls=%fused_computation.7 | convolution fusion | flops 68943872 | bytes 2637824 | tf_op jit(solution)/shard_map/bkgqs,bskd->bkgqd/dot_general | solution.py:53
  17.1 0.3 copy.47
  17.4 1.7 %convolution_convert_fusion = bf16[256,2048]{1,0:T(8,128)(2,1)} fusion(bf16[512,2048]{1,0:T(8,128)(2,1)S(1)} %copy-done, bf16[64,8,2,128]{3,2,1,0:T(2,128)(2,1)S(1)} %bitcast.75), kind=kOutput, calls=%fused_computation | convolution fusion | flops 537395200 | bytes 3407872 | tf_op jit(solution)/shard_map/dot_general | solution.py:410
  19.1 90.2 %shard_map.118 = bf16[64,2048]{1,0:T(8,128)(2,1)} custom-call(bf16[4,64,2048]{2,1,0:T(8,128)(2,1)} %bitcast.73, bf16[64,2048]{1,0:T(8,128)(2,1)} %resid.1, f32[1,2048]{1,0:T(1,128)} %bitcast.79, bf16[64,128]{1,0:T(8,128)(2,1)} %pad.4.extra, bf16[128,64]{1,0:T(8,128)(2,1)} %fusion.21.sel, bf16[64,128]{1,0:T(8,128)(2,1)} %fusion.23.sel_back, ...), custom_call_target="tpu_custom_call" | custom-call | tf_op jit(solution)/shard_map/pallas_call | solution.py:323
  109.3 1.7 %copy.67 = bf16[64,2048]{1,0:T(8,128)(2,1)} copy(bf16[64,2048]{1,0:T(8,128)(2,1)} %shard_map.118) | data formatting | bytes 524288
  (34 shorter events, 0.7 us)
Async XLA Ops:
  0.0 17.4 %copy-start = (bf16[512,2048]{1,0:T(8,128)(2,1)S(1)}, bf16[512,2048]{1,0:T(8,128)(2,1)}, u32[]{:S(2)}) copy-start(bf16[512,2048]{1,0:T(8,128)(2,1)} %param.17) | copy-start | bytes 6291460
  2.1 7.1 %copy-start.3 = (f32[8]{0:T(128)S(1)}, f32[8]{0:T(128)}, u32[]{:S(2)}) copy-start(f32[8]{0:T(128)} %param.15) | copy-start | bytes 100
  2.2 9.9 %collective-permute-start = (bf16[2,128,256]{1,2,0:T(8,128)(2,1)S(1)}, bf16[2,128,256]{1,2,0:T(8,128)(2,1)S(1)}, u32[]{:S(2)}, u32[]{:S(2)}) collective-permute-start(bf16[2,128,256]{1,2,0:T(8,128)(2,1)S(1)} %pad_maximum_fusion.2), channel_id=1, source_target_pairs={{0,4},{4,8},{8,12},{12,16},{16,20},{20,24},{24,28},{1,5},{5,9},{9,... | collective-permute-start | bytes 393224 | tf_op jit(solution)/shard_map/ppermute | solution.py:18
  12.3 2.4 %copy-start.2 = (bf16[256,256]{1,0:T(8,128)(2,1)S(1)}, bf16[256,256]{1,0:T(8,128)(2,1)}, u32[]{:S(2)}) copy-start(bf16[256,256]{1,0:T(8,128)(2,1)} %param.14) | copy-start | bytes 393220
  12.8 1.4 %copy-start.1 = (f32[2,4,2,128,256]{3,4,2,1,0:T(8,128)}, f32[2,4,2,128,256]{3,4,2,1,0:T(8,128)S(1)}, u32[]{:S(2)}) copy-start(f32[2,4,2,128,256]{3,4,2,1,0:T(8,128)S(1)} %get-tuple-element.20) | copy-start | bytes 6291460

commit v2 on v1

--- a/solution.py
+++ b/solution.py
@@ -162,129 +162,169 @@
     normed[:, width:] = extra[...]
 
     def block(tt, cc, zz):
-        return rows.at[tt, pl.ds(pl.multiple_of((cc * GROUPS + zz) * cap, cap), cap)]
+        return rows.at[zz, pl.ds(pl.multiple_of((cc * tp_n + tt) * cap, cap), cap)]
 
     def pack(g):
         s = sel[pl.ds(pl.multiple_of(g * cap, cap), cap), :]
         return jnp.dot(s, normed[...], preferred_element_type=jnp.float32).astype(jnp.bfloat16)
 
+    order = (0, 1, 3, 2)
+    ag = {}
+    pt = {}
+
+    def push(d, k, tt, to):
+        ref = block(tt, core, zoff(-k))
+        ag[(d, k)] = send(ref, ref, ag_s.at[d - 1, k], ag_r.at[d - 1, k], (sp, peer[to]))
+
+    def across(d, k):
+        ref = block(peer[d], core, zoff(-k))
+        pt[(d, k)] = send(ref, ref, pt_s.at[d, k], pt_r.at[d, k], (partner, t))
+
     disp = [None] * GROUPS
-    for k in (2, 1, 3):
+
+    def spread(i):
+        k = order[i]
+        if k:
+            disp[k].wait_recv()
+        push(1, k, t, 1)
+        push(2, k, t, 2)
+        across(0, k)
+
+    def relay(i):
+        k = order[i]
+        via = 1 + i % 2
+        ag[(via, k)].wait_recv()
+        push(3, k, peer[via], 3 - via)
+        across(via, k)
+        ag[(3 - via, k)].wait_recv()
+        across(3 - via, k)
+
+    def corner(i):
+        k = order[i]
+        ag[(3, k)].wait_recv()
+        across(3, k)
+
+    def widen(i):
+        k = order[i]
+        zz = zoff(-k)
+        for d in (0, 1, 2, 3):
+            pt[(d, k)].wait_recv()
+
+        @pl.loop(0, wg.shape[1] // TILE)
+        def _(n):
+            cols = pl.ds(pl.multiple_of(n * TILE, TILE), TILE)
+            x = rows[zz, :, :width]
+            g = jnp.dot(x, wg[:, cols], preferred_element_type=jnp.float32)
+            u = jnp.dot(x, wu[:, cols], preferred_element_type=jnp.float32)
+            hid[:, cols] = (g / (1.0 + jnp.exp(-g)) * u).astype(jnp.bfloat16)
+
+    swap = {}
+
+    def narrow(i):
+        k = order[i]
+        ext = rows[zoff(-k), :, width:].astype(jnp.float32)
+        lane = lax.broadcasted_iota(jnp.int32, ext.shape, 1)
+        mine = (lane == core) | (lane == core + 2)
+        weight = jnp.sum(jnp.where(mine, ext, 0.0), -1, keepdims=True)
+
+        @pl.loop(0, width // TILE)
+        def _(n):
+            cols = pl.ds(pl.multiple_of(n * TILE, TILE), TILE)
+            y = jnp.dot(hid[...], wd[:, cols], preferred_element_type=jnp.float32)
+            outp[k, :, cols] = (y * weight).astype(jnp.bfloat16)
+
+        other = outp.at[k, pl.ds(pl.multiple_of((1 - core) * half, half), half)]
+        swap[k] = send(other, pr.at[k], pr_s.at[k], pr_r.at[k], (partner, t))
+
+    def own(k, d):
+        off = pl.multiple_of((core * tp_n + peer[d]) * cap, cap)
+        here = pl.ds(pl.multiple_of(peer[d] * cap, cap), cap)
+        return outp[k, pl.ds(off, cap), :].astype(jnp.float32) + pr[k, here, :].astype(jnp.float32)
+
+    r2 = {}
+
+    def ship(k, d, to):
+        r2[(d, k)] = send(
+            comb.at[k, d - 1], rs2.at[k, d - 1],
+            r2_s.at[d - 1, k], r2_r.at[d - 1, k], (sp, peer[to]),
+        )
+
+    def combine(i):
+        k = order[i]
+        via = 1 + i % 2
+        swap[k].wait_recv()
+        comb[k, 2] = own(k, 3).astype(jnp.bfloat16)
+        ship(k, 3, via)
+        comb[k, via - 1] = own(k, via).astype(jnp.bfloat16)
+        ship(k, via, via)
+
+    def combine_on(i):
+        k = order[i]
+        on = 2 - i % 2
+        r2[(3, k)].wait_recv()
+        comb[k, on - 1] = (own(k, on) + rs2[k, 2].astype(jnp.float32)).astype(jnp.bfloat16)
+        ship(k, on, on)
+
+    bk = []
+
+    def finish(i):
+        k = order[i]
+        acc = own(k, 0)
+        for d in (1, 2):
+            r2[(d, k)].wait_recv()
+            acc = acc + rs2[k, d - 1].astype(jnp.float32)
+        if k:
+            ret[k] = acc.astype(jnp.bfloat16)
+            bk.append(
+                send(
+                    ret.at[k], back.at[z], bk_s.at[k - 1], bk_r.at[k - 1],
+                    (2 * zoff(-k) + core, t),
+                )
+            )
+        else:
+            back[z] = acc.astype(jnp.bfloat16)
+
+    block(t, core, z)[...] = pack(z)
+    spread(0)
+    for k in (1, 3, 2):
         g = zoff(k)
         outb[k] = pack(g)
         disp[k] = send(
             outb.at[k], block(t, core, z), di_s.at[k - 1], di_r.at[k - 1], (2 * g + core, t)
         )
-    block(t, core, z)[...] = pack(z)
-
-    ag = {}
-    pt = {}
-
-    def push(d, k, tt, to):
-        ref = block(tt, core, zoff(-k))
-        ag[(d, k)] = send(ref, ref, ag_s.at[d - 1, k], ag_r.at[d - 1, k], (sp, peer[to]))
-
-    def across(d, k):
-        ref = block(peer[d], core, zoff(-k))
-        pt[(d, k)] = send(ref, ref, pt_s.at[d, k], pt_r.at[d, k], (partner, t))
-
-    order = (0, 1, 3, 2)
-
-    def relay(i):
-        k = order[i]
-        ag[(1, k)].wait_recv()
-        if i < 2:
-            push(3, k, peer[1], 2)
-        across(1, k)
-        ag[(2, k)].wait_recv()
-        if i >= 2:
-            push(3, k, peer[2], 1)
-        across(2, k)
-
-    for i, k in enumerate(order):
-        if k:
-            disp[k].wait_recv()
-        push(1, k, t, 1)
-        push(2, k, t, 2)
-        across(0, k)
-        if i:
-            relay(i - 1)
-
+    relay(0)
+    corner(0)
+    spread(1)
     for c in loads:
         c.wait()
-
-    def experts(d):
-        for k in order:
-            pt[(d, k)].wait_recv()
-        tt = peer[d]
-
-        @pl.loop(0, wg.shape[1] // TILE)
-        def _(n):
-            cols = pl.ds(pl.multiple_of(n * TILE, TILE), TILE)
-            x = rows[tt, :, :width]
-            g = jnp.dot(x, wg[:, cols], preferred_element_type=jnp.float32)
-            u = jnp.dot(x, wu[:, cols], preferred_element_type=jnp.float32)
-            hid[:, cols] = (g / (1.0 + jnp.exp(-g)) * u).astype(jnp.bfloat16)
-
-        ext = rows[tt, :, width:].astype(jnp.float32)
-        lane = lax.broadcasted_iota(jnp.int32, ext.shape, 1)
-        mine = (lane == core) | (lane == core + 2)
-        weight = jnp.sum(jnp.where(mine, ext, 0.0), -1, keepdims=True)
-
-        @pl.loop(0, width // TILE)
-        def _(n):
-            cols = pl.ds(pl.multiple_of(n * TILE, TILE), TILE)
-            y = jnp.dot(hid[...], wd[:, cols], preferred_element_type=jnp.float32)
-            outp[d, :, cols] = (y * weight).astype(jnp.bfloat16)
-
-        src = outp.at[d, pl.ds(pl.multiple_of((1 - core) * half, half), half)]
-        return send(src, pr.at[d], pr_s.at[d], pr_r.at[d], (partner, t))
-
-    def own(d, zz):
-        off = pl.multiple_of((core * GROUPS + zz) * cap, cap)
-        here = pl.ds(pl.multiple_of(zz * cap, cap), cap)
-        return outp[d, pl.ds(off, cap), :].astype(jnp.float32) + pr[d, here, :].astype(jnp.float32)
-
-    back_order = (2, 1, 3, 0)
-    r2 = {}
-
-    def combine(d, swap):
-        swap.wait_recv()
-        for k in back_order:
-            zz = zoff(-k)
-            comb[d - 1, k] = own(d, zz).astype(jnp.bfloat16)
-            r2[(d, k)] = send(
-                comb.at[d - 1, k], rs2.at[d - 1, k],
-                r2_s.at[d - 1, k], r2_r.at[d - 1, k], (sp, peer[d]),
-            )
-
-    swap0 = experts(0)
+    widen(0)
+    relay(1)
+    spread(2)
+    narrow(0)
+    corner(1)
+    widen(1)
+    relay(2)
+    spread(3)
+    combine(0)
+    narrow(1)
+    corner(2)
+    widen(2)
     relay(3)
-    swap1 = experts(1)
-    swap0.wait_recv()
-    for k in order:
-        ag[(3, k)].wait_recv()
-        across(3, k)
-    combine(1, swap1)
-    swap2 = experts(2)
-    combine(2, swap2)
-    swap3 = experts(3)
-    combine(3, swap3)
-
-    bk = []
-    for k in back_order:
-        zz = zoff(-k)
-        acc = own(0, zz)
-        for d in (1, 2, 3):
-            r2[(d, k)].wait_recv()
-            acc = acc + rs2[d - 1, k].astype(jnp.float32)
-        if k:
-            ret[k] = acc.astype(jnp.bfloat16)
-            bk.append(
-                send(ret.at[k], back.at[z], bk_s.at[k - 1], bk_r.at[k - 1], (2 * zz + core, t))
-            )
-        else:
-            back[z] = acc.astype(jnp.bfloat16)
+    combine_on(0)
+    combine(1)
+    narrow(2)
+    corner(3)
+    combine_on(1)
+    widen(3)
+    finish(0)
+    combine(2)
+    narrow(3)
+    finish(1)
+    combine_on(2)
+    combine(3)
+    finish(2)
+    combine_on(3)
+    finish(3)
     for c in bk:
         c.wait_recv()
     routed = jnp.dot(
@@ -336,7 +376,7 @@
             pltpu.VMEM((row_n, width), bf),
             pltpu.VMEM((row_n, ext_width), bf),
             pltpu.VMEM((GROUPS, cap, ext_width), bf),
-            pltpu.VMEM((tp_n, 2 * half, ext_width), bf),
+            pltpu.VMEM((GROUPS, 2 * half, ext_width), bf),
             dma((3,)),
             dma((3,)),
             dma((3, GROUPS)),
@@ -348,8 +388,8 @@
             pltpu.VMEM((4, half, width), bf),
             dma((4,)),
             dma((4,)),
-            pltpu.VMEM((3, GROUPS, cap, width), bf),
-            pltpu.VMEM((3, GROUPS, cap, width), bf),
+            pltpu.VMEM((GROUPS, 3, cap, width), bf),
+            pltpu.VMEM((GROUPS, 3, cap, width), bf),
             dma((3, GROUPS)),
             dma((3, GROUPS)),
             pltpu.VMEM((GROUPS, cap, width), bf),

time: 113 us -> 109 us (0.965); the launches traced: 111 us -> 108 us
  Pallas kernels: 90.2 us -> 87.5 us
    pallas_call x1, Pallas kernels: 90.2 us -> 87.5 us  [group_experts(): pl.pallas_call(group_kernel, out_shape=jax.ShapeDtypeStruct((row_n, width...]
where the time goes in v2:
time: 109 us; the launch traced here: 108 us
  Pallas kernels  87.5 us (80%)
  local copies, waits for them, and re-layouts  9.82 us (9%)
  matrix products  4.3 us (4%)
  other arithmetic  3.97 us (4%)
  starting transfers between devices  2.4 us (2%)
    pallas_call x1, Pallas kernels, group_experts(): pl.pallas_call(group_kernel, out_shape=jax.ShapeDtypeStruct((row_n, width...  87.5 us
    unnamed x12, local copies, waits for them, and re-layouts  5.3 us
    ppermute x1, starting transfers between devices, from_behind(): return lax.ppermute(block, axis, route)  2.4 us
  transfers between devices with their start and end apart: 1, of which 0 were waited for; matrix products, arithmetic and copies ran while one was open for 7% of the time, Pallas kernels for 0%

profile of v2, /device:TPU:0, one launch (start us, length us, event | category | flops | bytes accessed | tf_op | source)
XLA Modules:
  0.0 108.3 jit_solution(1445413925044406356)
XLA Ops:
  0.0 1.1 %copy.33 = bf16[256,256]{0,1:T(8,128)(2,1)S(1)} copy(bf16[256,256]{1,0:T(8,128)(2,1)} %param.13) | data formatting | bytes 262144 | tf_op args[1]
  1.2 0.8 slice.50
  2.0 0.1 copy.56
  2.2 2.4 %collective-permute-start = (bf16[2,128,256]{1,2,0:T(8,128)(2,1)S(1)}, bf16[2,128,256]{1,2,0:T(8,128)(2,1)S(1)}, u32[]{:S(2)}, u32[]{:S(2)}) collective-permute-start(bf16[2,128,256]{1,2,0:T(8,128)(2,1)S(1)} %pad_maximum_fusion.2), channel_id=1, source_target_pairs={{0,4},{4,8},{8,12},{12,16},{16,20},{20,24},{24,28},{1,5},{5,9},{9,... | collective-permute-start | bytes 393224 | tf_op jit(solution)/shard_map/ppermute | solution.py:18
  4.7 1.1 reshape.239
  5.8 0.8 fusion.24
  6.6 0.8 constant_dynamic-slice_fusion
  7.4 0.3 multiply_cosine_fusion
  7.6 0.2 multiply_cosine_fusion.1
  7.8 1.1 %copy.38 = bf16[256,512]{0,1:T(8,128)(2,1)S(1)} copy(bf16[256,512]{1,0:T(8,128)(2,1)} %param.12) | data formatting | bytes 524288 | tf_op args[0]
  9.0 0.1 subtract_convert_fusion
  9.3 0.1 max.19
  9.3 0.2 copy.45
  9.5 0.1 copy.48
  9.7 0.1 reduce_window_sum.11
  9.8 0.2 select_reduce_fusion
  10.0 0.6 fusion.21.sel
  10.6 0.1 broadcast_and_fusion
  10.8 0.6 pad.4.extra
  11.4 0.7 fusion.23.sel_back
  12.3 0.5 fusion.31
  12.9 1.3 %copy-done.1 = f32[2,4,2,128,256]{3,4,2,1,0:T(8,128)} copy-done((f32[2,4,2,128,256]{3,4,2,1,0:T(8,128)}, f32[2,4,2,128,256]{3,4,2,1,0:T(8,128)S(1)}, u32[]{:S(2)}) %copy-start.1) | copy-done | bytes 2097176
  14.2 0.3 fusion
  14.5 0.1 add_bitcast_fusion
  14.6 0.1 copy.41
  14.7 0.2 reshape.238
  14.9 0.2 copy.44
  15.1 2.1 %fusion.3 = bf16[2,128,4,2,64]{1,4,3,2,0:T(8,128)(2,1)S(1)} fusion(f32[2,4,2,128,256]{3,4,2,1,0:T(8,128)} %copy-done.1, f32[2,4,2,128]{3,2,1,0:T(2,128)S(1)} %broadcast_maximum_fusion, bf16[2,128,4,64]{1,3,2,0:T(8,128)(2,1)S(1)} %copy.45, bf16[2,128,4,64]{1,3,2,0:T(8,128)(2,1)S(1)} %copy.44, f32[2,128,4,2]{1,3,2,0:T(2,128)S(1)} %add_bitcast_fusion), kind=kOutput, calls=%fused_computation.7 | convolution fusion | flops 68943872 | bytes 2637824 | tf_op jit(solution)/shard_map/bkgqs,bskd->bkgqd/dot_general | solution.py:53
  17.1 0.3 copy.47
  17.4 1.7 %convolution_convert_fusion = bf16[256,2048]{1,0:T(8,128)(2,1)} fusion(bf16[512,2048]{1,0:T(8,128)(2,1)S(1)} %copy-done, bf16[64,8,2,128]{3,2,1,0:T(2,128)(2,1)S(1)} %bitcast.75), kind=kOutput, calls=%fused_computation | convolution fusion | flops 537395200 | bytes 3407872 | tf_op jit(solution)/shard_map/dot_general | solution.py:450
  19.1 87.5 %shard_map.118 = bf16[64,2048]{1,0:T(8,128)(2,1)} custom-call(bf16[4,64,2048]{2,1,0:T(8,128)(2,1)} %bitcast.73, bf16[64,2048]{1,0:T(8,128)(2,1)} %resid.1, f32[1,2048]{1,0:T(1,128)} %bitcast.79, bf16[64,128]{1,0:T(8,128)(2,1)} %pad.4.extra, bf16[128,64]{1,0:T(8,128)(2,1)} %fusion.21.sel, bf16[64,128]{1,0:T(8,128)(2,1)} %fusion.23.sel_back, ...), custom_call_target="tpu_custom_call" | custom-call | tf_op jit(solution)/shard_map/pallas_call | solution.py:363
  106.6 1.7 %copy.67 = bf16[64,2048]{1,0:T(8,128)(2,1)} copy(bf16[64,2048]{1,0:T(8,128)(2,1)} %shard_map.118) | data formatting | bytes 524288
  (34 shorter events, 0.7 us)
Async XLA Ops:
  0.0 17.4 %copy-start = (bf16[512,2048]{1,0:T(8,128)(2,1)S(1)}, bf16[512,2048]{1,0:T(8,128)(2,1)}, u32[]{:S(2)}) copy-start(bf16[512,2048]{1,0:T(8,128)(2,1)} %param.17) | copy-start | bytes 6291460
  2.1 7.1 %copy-start.3 = (f32[8]{0:T(128)S(1)}, f32[8]{0:T(128)}, u32[]{:S(2)}) copy-start(f32[8]{0:T(128)} %param.15) | copy-start | bytes 100
  2.2 9.9 %collective-permute-start = (bf16[2,128,256]{1,2,0:T(8,128)(2,1)S(1)}, bf16[2,128,256]{1,2,0:T(8,128)(2,1)S(1)}, u32[]{:S(2)}, u32[]{:S(2)}) collective-permute-start(bf16[2,128,256]{1,2,0:T(8,128)(2,1)S(1)} %pad_maximum_fusion.2), channel_id=1, source_target_pairs={{0,4},{4,8},{8,12},{12,16},{16,20},{20,24},{24,28},{1,5},{5,9},{9,... | collective-permute-start | bytes 393224 | tf_op jit(solution)/shard_map/ppermute | solution.py:18
  12.3 2.4 %copy-start.2 = (bf16[256,256]{1,0:T(8,128)(2,1)S(1)}, bf16[256,256]{1,0:T(8,128)(2,1)}, u32[]{:S(2)}) copy-start(bf16[256,256]{1,0:T(8,128)(2,1)} %param.14) | copy-start | bytes 393220
  12.8 1.4 %copy-start.1 = (f32[2,4,2,128,256]{3,4,2,1,0:T(8,128)}, f32[2,4,2,128,256]{3,4,2,1,0:T(8,128)S(1)}, u32[]{:S(2)}) copy-start(f32[2,4,2,128,256]{3,4,2,1,0:T(8,128)S(1)} %get-tuple-element.20) | copy-start | bytes 6291460
